TPU v7x, 32 devices: a whole 2x2x4 slice. The times are simulated.
32 devices in a mesh: kv: 8 (over z, y), tp: 4 (over x, core).
Axes of the slice: x: 2, y: 2, z: 4, core: 2. Of those that a mesh axis runs over, the one named last changes fastest.
Arguments:
- tokens: bfloat16 [32, 4096], P(None, 'kv'), may hold values from -8 to 8, as said below
- attn_gain: float32 [4096], P('kv'), may hold values from 0.1 to 1.9
- query_weight: bfloat16 [4096, 1024], P('kv', 'tp'), may hold values from -0.09375 to 0.09375
- key_weight: bfloat16 [4096, 1024], P('kv', 'tp'), may hold values from -0.09375 to 0.09375
- value_weight: bfloat16 [4096, 2048], P('kv', 'tp'), may hold values from -0.09375 to 0.09375
- outgate_weight: bfloat16 [4096, 2048], P('kv', 'tp'), may hold values from -0.09375 to 0.09375
- code_weight: bfloat16 [4096, 16], P('kv'), may hold values from -0.09375 to 0.09375
- decay_weight: bfloat16 [16, 1024], P(None, 'tp'), may hold values from -6 to 6
- decay_bias: float32 [1024], P('tp'), may hold values from -4 to 2
- head_gain: float32 [256], replicated, may hold values from 0.1 to 1.9
- key_cache: bfloat16 [32, 64, 8, 128], P('kv', None, 'tp'), may hold values from -6 to 6
- value_cache: bfloat16 [32, 64, 8, 256], P('kv', None, 'tp'), may hold values from -6 to 6
- decay_cache: float32 [32, 64, 8, 128], P('kv', None, 'tp'), may hold values from -1.1 to 0
- carried_state: float32 [32, 8, 128, 256], P('kv', 'tp'), may hold values from -24 to 24
- lengths: int32 [32], P('kv'), may hold values from 1 to 64, 832 in all
- output_weight: bfloat16 [2048, 4096], P('tp', 'kv'), may hold values from -0.125 to 0.125
- mlp_gain: float32 [4096], P('kv'), may hold values from 0.1 to 1.9
- gate_weight: bfloat16 [4096, 11008], P('kv', 'tp'), may hold values from -0.09375 to 0.09375
- up_weight: bfloat16 [4096, 11008], P('kv', 'tp'), may hold values from -0.09375 to 0.09375
- down_weight: bfloat16 [11008, 4096], P('tp', 'kv'), may hold values from -0.0546875 to 0.0546875
Outputs:
- layer_out: bfloat16 [32, 4096], P(None, 'kv')
- new_keys: bfloat16 [32, 8, 128], P('kv', 'tp')
- new_values: bfloat16 [32, 8, 256], P('kv', 'tp')
Inputs may be any that keep to these rules, and one draw needn't show every extreme that they name: `tokens`: the features of a row have unlike scales. Sequence b's new token comes right after its lengths[b] live positions; positions from lengths[b] on take no part.
All inputs are finite; a program needn't handle non-finite values. No bound on the sum of `lengths` on one device may be relied on, other than what follows from the above.
Results may differ from a plain program's by a relative error of at most 0.025.
Values may be sent and summed in bfloat16 or wider, within the bound.
A program may use at most 64 MiB of HBM per device.

v0:
```python
import jax
import jax.numpy as jnp
from jax import lax
from jax.sharding import PartitionSpec as P

WIDTH = 4096
EPS = 1e-06
GATE_TEMP = 16.0


def across_heads(partial_value):
    return lax.psum(partial_value.astype(jnp.bfloat16), "tp").astype(jnp.float32)


def block_attention(
    queries,
    new_keys,
    new_values,
    new_decay,
    key_cache,
    value_cache,
    decay_cache,
    carried_state,
    lengths,
):
    positions = jnp.arange(key_cache.shape[1], dtype=jnp.int32)
    live_mask = positions[None, :] < lengths[:, None]
    kept_decay = jnp.where(live_mask[:, :, None, None], decay_cache, jnp.zeros_like(decay_cache))
    later_sum = lax.cumsum(kept_decay, axis=1, reverse=True) - kept_decay
    total_decay = jnp.sum(kept_decay, axis=1)
    decayed = queries.astype(jnp.float32) * jnp.exp(new_decay)
    carried = jnp.einsum(
        "bhd,bhde->bhe",
        decayed * jnp.exp(total_decay),
        carried_state,
        precision=lax.Precision.HIGHEST,
    )
    keyed_cache = key_cache.astype(jnp.float32) * jnp.exp(later_sum)
    scores = jnp.einsum("bhd,bshd->bhs", decayed, keyed_cache, precision=lax.Precision.HIGHEST)
    scores = jnp.where(live_mask[:, None, :], scores, jnp.zeros_like(scores)).astype(jnp.bfloat16)
    within = jnp.einsum("bhs,bshe->bhe", scores, value_cache, preferred_element_type=jnp.float32)
    own_score = jnp.sum(queries.astype(jnp.float32) * new_keys.astype(jnp.float32), axis=-1)
    return carried + within + own_score[..., None] * new_values.astype(jnp.float32)


def mixer_hidden(gate_sum, up_sum, square_sum):
    inv_mid = lax.rsqrt(square_sum / WIDTH + EPS)[:, None]
    return (jax.nn.silu(gate_sum * inv_mid) * (up_sum * inv_mid)).astype(jnp.bfloat16)


def on_device(
    tokens,
    attn_gain,
    query_weight,
    key_weight,
    value_weight,
    outgate_weight,
    code_weight,
    decay_weight,
    decay_bias,
    head_gain,
    key_cache,
    value_cache,
    decay_cache,
    carried_state,
    lengths,
    output_weight,
    mlp_gain,
    gate_weight,
    up_weight,
    down_weight,
):
    local_seqs, heads_here, key_dim, value_dim = carried_state.shape
    token_f = tokens.astype(jnp.float32)
    scaled = (token_f * attn_gain[None, :]).astype(jnp.bfloat16)
    query_part = jnp.dot(scaled, query_weight, preferred_element_type=jnp.float32)
    key_part = jnp.dot(scaled, key_weight, preferred_element_type=jnp.float32)
    value_part = jnp.dot(scaled, value_weight, preferred_element_type=jnp.float32)
    outgate_part = jnp.dot(scaled, outgate_weight, preferred_element_type=jnp.float32)
    code_part = jnp.dot(scaled, code_weight, preferred_element_type=jnp.float32)
    token_squares = jnp.sum(token_f * token_f, axis=1)
    query_sum, key_sum, value_sum, outgate_sum, code_sum, square_sum = (
        lax.psum_scatter(
            query_part.astype(jnp.bfloat16), "kv", scatter_dimension=0, tiled=True
        ).astype(jnp.float32),
        lax.psum_scatter(
            key_part.astype(jnp.bfloat16), "kv", scatter_dimension=0, tiled=True
        ).astype(jnp.float32),
        lax.psum_scatter(
            value_part.astype(jnp.bfloat16), "kv", scatter_dimension=0, tiled=True
        ).astype(jnp.float32),
        lax.psum_scatter(
            outgate_part.astype(jnp.bfloat16), "kv", scatter_dimension=0, tiled=True
        ).astype(jnp.float32),
        lax.psum_scatter(
            code_part.astype(jnp.bfloat16), "kv", scatter_dimension=0, tiled=True
        ).astype(jnp.float32),
        lax.psum_scatter(
            token_squares.astype(jnp.bfloat16), "kv", scatter_dimension=0, tiled=True
        ).astype(jnp.float32),
    )
    inv_rms = lax.rsqrt(square_sum / WIDTH + EPS)[:, None]
    queries = (
        (query_sum * inv_rms * key_dim ** (-0.5))
        .astype(jnp.bfloat16)
        .reshape(local_seqs, heads_here, key_dim)
    )
    new_keys = (key_sum * inv_rms).astype(jnp.bfloat16).reshape(local_seqs, heads_here, key_dim)
    new_values = (
        (value_sum * inv_rms).astype(jnp.bfloat16).reshape(local_seqs, heads_here, value_dim)
    )
    out_gate = (
        (outgate_sum * inv_rms).astype(jnp.bfloat16).reshape(local_seqs, heads_here, value_dim)
    )
    gate_code = (code_sum * inv_rms).astype(jnp.bfloat16)
    pre_gate = (
        jnp.dot(gate_code, decay_weight, preferred_element_type=jnp.float32) + decay_bias[None, :]
    )
    new_decay = (jax.nn.log_sigmoid(pre_gate) / GATE_TEMP).reshape(local_seqs, heads_here, key_dim)
    mixed_heads = block_attention(
        queries,
        new_keys,
        new_values,
        new_decay,
        key_cache,
        value_cache,
        decay_cache,
        carried_state,
        lengths,
    )
    normed = (
        mixed_heads
        * lax.rsqrt(jnp.mean(mixed_heads * mixed_heads, axis=-1, keepdims=True) + EPS)
        * head_gain
    )
    heads_out = (
        (normed * jax.nn.silu(out_gate.astype(jnp.float32)))
        .astype(jnp.bfloat16)
        .reshape(local_seqs, heads_here * value_dim)
    )
    attended = across_heads(
        jnp.dot(
            lax.all_gather(heads_out, "kv", axis=0, tiled=True),
            output_weight,
            preferred_element_type=jnp.float32,
        )
    )
    middle = (token_f + attended).astype(jnp.bfloat16)
    mid_f = middle.astype(jnp.float32)
    scaled_mid = (mid_f * mlp_gain[None, :]).astype(jnp.bfloat16)
    gate_part = jnp.dot(scaled_mid, gate_weight, preferred_element_type=jnp.float32)
    up_part = jnp.dot(scaled_mid, up_weight, preferred_element_type=jnp.float32)
    mid_squares = jnp.sum(mid_f * mid_f, axis=1)
    gate_sum, up_sum, mid_sum = (
        lax.psum(gate_part.astype(jnp.bfloat16), "kv").astype(jnp.float32),
        lax.psum(up_part.astype(jnp.bfloat16), "kv").astype(jnp.float32),
        lax.psum(mid_squares.astype(jnp.bfloat16), "kv").astype(jnp.float32),
    )
    hidden = mixer_hidden(gate_sum, up_sum, mid_sum)
    lifted_part = jnp.dot(hidden, down_weight, preferred_element_type=jnp.float32)
    layer_out = (mid_f + across_heads(lifted_part)).astype(jnp.bfloat16)
    return (layer_out, new_keys, new_values)


def solution(mesh):
    in_specs = (
        P(None, "kv"),
        P("kv"),
        P("kv", "tp"),
        P("kv", "tp"),
        P("kv", "tp"),
        P("kv", "tp"),
        P("kv", None),
        P(None, "tp"),
        P("tp"),
        P(),
        P("kv", None, "tp", None),
        P("kv", None, "tp", None),
        P("kv", None, "tp", None),
        P("kv", "tp", None, None),
        P("kv"),
        P("tp", "kv"),
        P("kv"),
        P("kv", "tp"),
        P("kv", "tp"),
        P("tp", "kv"),
    )
    out_specs = (P(None, "kv"), P("kv", "tp", None), P("kv", "tp", None))
    return jax.shard_map(
        on_device, mesh=mesh, in_specs=in_specs, out_specs=out_specs, check_vma=False
    )
```

profile of v0, /device:TPU:0, one launch (start us, length us, event | category | flops | bytes accessed | tf_op | source)
XLA Modules:
  0.0 236.8 jit_solution(11415016828430029316)
XLA Ops:
  7.3 1.5 fusion.11
  8.8 1.5 convolution_convert_fusion.8
  10.3 1.7 convolution_convert_fusion.7
  12.1 1.7 convolution_convert_fusion.6
  13.8 1.9 convolution_convert_fusion.5
  15.7 1.9 convolution_convert_fusion.4
  18.4 1.2 dynamic-slice
  20.3 2.6 %exponential_multiply_fusion = f32[4,64,2,128]{3,2,1,0:T(2,128)S(1)} fusion(bf16[4,64,2,128]{3,2,1,0:T(2,128)(2,1)} %param.30, f32[4,64,2,128]{3,2,1,0:T(2,128)} %param.32, pred[4,64]{1,0:T(4,128)(4,1)S(1)} %iota_compare_fusion), kind=kOutput, calls=%fused_computation.16 | output fusion | flops 4456448 | bytes 655616 | tf_op jit(solution)/shard_map/block_attention/reduce_window_sum | solution.py:29
  23.2 68.5 %all-reduce.11.cloned.1.call-done = (bf16[32,512]{1,0:T(8,128)(2,1)}, bf16[32]{0:T(256)(128)(2,1)}, bf16[32,256]{1,0:T(8,128)(2,1)}, bf16[32,16]{1,0:T(8,128)(2,...) async-done(((bf16[32,512]{1,0:T(8,128)(2,1)}, bf16[32]{0:T(256)(128)(2,1)}, bf16[32,256]{1,0:T(8,128)(2,1)}, bf16[32,16]{1,0:T(8,128)(2,1)}, ...) | async-done | bytes 99408
  91.8 0.7 fusion.36
  92.5 0.9 fusion.29
  93.4 0.8 multiply_convert_fusion.4
  94.2 0.8 multiply_convert_fusion.3
  95.6 1.8 fusion.41
  97.5 1.1 fusion.1
  98.9 30.6 %all-gather = bf16[8,4,512]{2,1,0:T(4,128)(2,1)S(1)} all-gather(bf16[1,4,512]{2,1,0:T(4,128)(2,1)S(1)} %reshape.79), channel_id=1, replica_groups=mesh['kv'=8,'tp'=4] {'kv'}, dimensions={0}, use_global_device_ids=true | all-gather | bytes 36864 | tf_op jit(solution)/shard_map/all_gather | solution.py:143
  129.5 1.2 convolution_convert_fusion.3
  130.7 10.3 %psum.35 = bf16[32,512]{1,0:T(8,128)(2,1)S(1)} all-reduce(bf16[32,512]{1,0:T(8,128)(2,1)S(1)} %convolution_convert_fusion.3), channel_id=1, replica_groups=mesh['kv'=8,'tp'=4] {'tp'}, use_global_device_ids=true, to_apply=%region_11.12 | all-reduce | flops 16384 | bytes 65536 | tf_op jit(solution)/shard_map/psum | solution.py:12
  141.2 1.6 convolution_convert_fusion
  142.8 1.6 convolution_convert_fusion.1
  144.4 20.6 %psum.37 = bf16[32]{0:T(256)(128)(2,1)S(1)} all-reduce(bf16[32]{0:T(256)(128)(2,1)S(1)} %get-tuple-element.11), channel_id=1, replica_groups=mesh['kv'=8,'tp'=4] {'kv'}, use_global_device_ids=true, to_apply=%region_14.15 | all-reduce | flops 32 | bytes 128 | tf_op jit(solution)/shard_map/psum | solution.py:157
  165.1 51.4 %all-reduce.13.cloned.1.call-done = (bf16[32,2752]{1,0:T(8,128)(2,1)}, bf16[32,2752]{1,0:T(8,128)(2,1)}) async-done(((bf16[32,2752]{1,0:T(8,128)(2,1)}, bf16[32,2752]{1,0:T(8,128)(2,1)}), (bf16[32,2752]{1,0:T(8,128)(2,1)}, bf16[32,2752]{1,0:T(8,128)(2,1)})) %all-reduce.13.cloned.1.call-update) | async-done | bytes 352272 | tf_op jit(solution)/shard_map/psum | solution.py:156
  216.4 2.6 %convolution_convert_fusion.2 = bf16[32,512]{1,0:T(8,128)(2,1)S(1)} fusion(bf16[2752,512]{1,0:T(8,128)(2,1)} %param.39, bf16[32,2752]{1,0:T(8,128)(2,1)} %get-tuple-element.9, bf16[32,2752]{1,0:T(8,128)(2,1)} %get-tuple-element.10, f32[32]{0:T(128)S(1)} %add_rsqrt_fusion.1), kind=kOutput, calls=%fused_computation.2 | convolution fusion | flops 91074560 | bytes 3203200 | tf_op jit(solution)/shard_map/dot_general | solution.py:160
  219.1 10.3 %psum.39 = bf16[32,512]{1,0:T(8,128)(2,1)S(1)} all-reduce(bf16[32,512]{1,0:T(8,128)(2,1)S(1)} %convolution_convert_fusion.2), channel_id=1, replica_groups=mesh['kv'=8,'tp'=4] {'tp'}, use_global_device_ids=true, to_apply=%region_16.17 | all-reduce | flops 16384 | bytes 65536 | tf_op jit(solution)/shard_map/psum | solution.py:12
  (42 shorter events, 3.0 us)
Async XLA Ops:
  7.2 134.0 %copy-start = (bf16[512,2752]{0,1:T(8,128)(2,1)S(1)}, bf16[512,2752]{0,1:T(8,128)(2,1)}, u32[]{:S(2)}) copy-start(bf16[512,2752]{0,1:T(8,128)(2,1)} %param.38) | copy-start | bytes 8454148
  7.2 15.7 %copy-start.2 = (f32[4,64,2,128]{3,2,1,0:T(2,128)S(1)}, f32[4,64,2,128]{3,2,1,0:T(2,128)}, u32[]{:S(2)}) copy-start(f32[4,64,2,128]{3,2,1,0:T(2,128)} %param.32) | copy-start | bytes 786436
  7.2 85.3 %copy-start.9 = (f32[256]{0:T(256)S(1)}, f32[256]{0:T(256)}, u32[]{:S(2)}) copy-start(f32[256]{0:T(256)} %param.28) | copy-start | bytes 3076
  7.2 85.3 %copy-start.8 = (bf16[16,256]{1,0:T(8,128)(2,1)S(1)}, bf16[16,256]{1,0:T(8,128)(2,1)}, u32[]{:S(2)}) copy-start(bf16[16,256]{1,0:T(8,128)(2,1)} %param.27) | copy-start | bytes 24580
  7.2 91.5 %copy-start.7 = (f32[256]{0:T(256)S(1)}, f32[256]{0:T(256)}, u32[]{:S(2)}) copy-start(f32[256]{0:T(256)} %param.29) | copy-start | bytes 3076
  7.2 84.6 %all-reduce.11.cloned.1.call-start = ((), (), s32[]{:S(2)}) async-start(), calls=%async_computation | async-start | bytes 214016
  10.3 130.7 %copy-start.3 = (bf16[32,512]{1,0:T(8,128)(2,1)S(1)}, bf16[32,512]{1,0:T(8,128)(2,1)}, u32[]{:S(2)}) copy-start(bf16[32,512]{1,0:T(8,128)(2,1)} %param.20) | copy-start | bytes 98308
  12.0 129.1 %copy-start.6 = (f32[512]{0:T(512)S(1)}, f32[512]{0:T(512)}, u32[]{:S(2)}) copy-start(f32[512]{0:T(512)} %param.36) | copy-start | bytes 6148
  17.6 198.9 %all-reduce.13.cloned.1.call-start = ((), (), s32[]{:S(2)}) async-start(), calls=%async_computation.1 | async-start | bytes 720896 | tf_op jit(solution)/shard_map/psum | solution.py:156
  94.2 48.6 %copy-start.5 = (bf16[4,2,128]{2,1,0:T(2,128)(2,1)}, bf16[4,2,128]{2,1,0:T(2,128)(2,1)S(1)}, u32[]{:S(2)}) copy-start(bf16[4,2,128]{2,1,0:T(2,128)(2,1)S(1)} %reshape.74) | copy-start | bytes 6148
  95.0 47.8 %copy-start.4 = (bf16[4,2,256]{2,1,0:T(2,128)(2,1)}, bf16[4,2,256]{2,1,0:T(2,128)(2,1)S(1)}, u32[]{:S(2)}) copy-start(bf16[4,2,256]{2,1,0:T(2,128)(2,1)S(1)} %reshape.75) | copy-start | bytes 12292
  141.0 1.8 copy-start.1
Sparse Core Ops, SparseCore 0:
  17.7 74.0 all-reduce.10
  144.6 71.8 all-reduce.12
where the time goes:
time: 238 us; the launch traced here: 237 us
  waiting for transfers between devices  120 us (50%)
  blocking collectives  71.8 us (30%)
  matrix products  20.1 us (8%)
  between operations  14.8 us (6%)
  other arithmetic  8.62 us (4%)
    unnamed x3, waiting for transfers between devices  68.6 us
    psum x1, waiting for transfers between devices, on_device(): lax.psum(up_part.astype(jnp.bfloat16), 'kv').astype(jnp.float32)  51.4 us
    all_gather x1, blocking collectives, on_device(): lax.all_gather(heads_out, 'kv', axis=0, tiled=True)  30.6 us
    psum x1, blocking collectives, on_device(): lax.psum(mid_squares.astype(jnp.bfloat16), 'kv').astype(jnp.float32)  20.6 us
    psum x2, blocking collectives, across_heads(): lax.psum(partial_value.astype(jnp.bfloat16), 'tp').astype(jnp.float32)  20.5 us
  transfers between devices with their start and end apart: 2, of which 2 were waited for; matrix products, arithmetic and copies ran while one was open for 2% of the time, Pallas kernels for 0%

commit v1 on v0

--- a/solution.py
+++ b/solution.py
@@ -9,7 +9,9 @@
 
 
 def across_heads(partial_value):
-    return lax.psum(partial_value.astype(jnp.bfloat16), "tp").astype(jnp.float32)
+    return jnp.sum(lax.all_gather(partial_value.astype(jnp.bfloat16), "tp"), axis=0).astype(
+        jnp.float32
+    )
 
 
 def block_attention(

time: 238 us -> 228 us (0.958)
  blocking collectives: 71.8 us -> 62.1 us
    psum x2 -> x0, blocking collectives: 20.5 us -> none  [across_heads(): lax.psum(partial_value.astype(jnp.bfloat16), 'tp').astype(jnp.float32)]
    all_gather x0 -> x2, blocking collectives: none -> 10.8 us  [across_heads(): lax.all_gather(partial_value.astype(jnp.bfloat16), 'tp')]
where the time goes in v1:
time: 228 us; the launch traced here: 227 us
  waiting for transfers between devices  120 us (53%)
  blocking collectives  62.1 us (27%)
  matrix products  20.1 us (9%)
  between operations  14.8 us (6%)
  other arithmetic  8.66 us (4%)
    unnamed x3, waiting for transfers between devices  68.6 us
    psum x1, waiting for transfers between devices, on_device(): lax.psum(up_part.astype(jnp.bfloat16), 'kv').astype(jnp.float32)  51.3 us
    all_gather x1, blocking collectives, on_device(): lax.all_gather(heads_out, 'kv', axis=0, tiled=True)  30.6 us
    psum x1, blocking collectives, on_device(): lax.psum(mid_squares.astype(jnp.bfloat16), 'kv').astype(jnp.float32)  20.6 us
    all_gather x2, blocking collectives, across_heads(): lax.all_gather(partial_value.astype(jnp.bfloat16), 'tp')  10.8 us
  transfers between devices with their start and end apart: 2, of which 2 were waited for; matrix products, arithmetic and copies ran while one was open for 2% of the time, Pallas kernels for 0%

profile of v1, /device:TPU:0, one launch (start us, length us, event | category | flops | bytes accessed | tf_op | source)
XLA Modules:
  0.0 227.1 jit_solution(13146004234326946709)
XLA Ops:
  7.3 1.5 fusion.11
  8.8 1.5 convolution_convert_fusion.8
  10.3 1.7 convolution_convert_fusion.7
  12.0 1.7 convolution_convert_fusion.6
  13.8 1.9 convolution_convert_fusion.5
  15.7 1.9 convolution_convert_fusion.4
  18.4 1.2 dynamic-slice
  20.3 2.6 %exponential_multiply_fusion = f32[4,64,2,128]{3,2,1,0:T(2,128)S(1)} fusion(bf16[4,64,2,128]{3,2,1,0:T(2,128)(2,1)} %param.30, f32[4,64,2,128]{3,2,1,0:T(2,128)} %param.32, pred[4,64]{1,0:T(4,128)(4,1)S(1)} %iota_compare_fusion), kind=kOutput, calls=%fused_computation.16 | output fusion | flops 4456448 | bytes 655616 | tf_op jit(solution)/shard_map/block_attention/reduce_window_sum | solution.py:31
  23.2 68.5 %all-reduce.11.cloned.1.call-done = (bf16[32,512]{1,0:T(8,128)(2,1)}, bf16[32]{0:T(256)(128)(2,1)}, bf16[32,256]{1,0:T(8,128)(2,1)}, bf16[32,16]{1,0:T(8,128)(2,...) async-done(((bf16[32,512]{1,0:T(8,128)(2,1)}, bf16[32]{0:T(256)(128)(2,1)}, bf16[32,256]{1,0:T(8,128)(2,1)}, bf16[32,16]{1,0:T(8,128)(2,1)}, ...) | async-done | bytes 99408
  91.8 0.7 fusion.36
  92.5 0.9 fusion.29
  93.4 0.8 multiply_convert_fusion.4
  94.2 0.8 multiply_convert_fusion.3
  95.6 1.8 fusion.41
  97.5 1.1 fusion.1
  98.9 30.6 %all-gather.2 = bf16[8,4,512]{2,1,0:T(4,128)(2,1)S(1)} all-gather(bf16[1,4,512]{2,1,0:T(4,128)(2,1)S(1)} %reshape.81), channel_id=1, replica_groups=mesh['kv'=8,'tp'=4] {'kv'}, dimensions={0}, use_global_device_ids=true | all-gather | bytes 36864 | tf_op jit(solution)/shard_map/all_gather | solution.py:145
  129.5 1.2 convolution_convert_fusion.3
  130.7 5.4 %all-gather = bf16[128,512]{1,0:T(8,128)(2,1)S(1)} all-gather(bf16[32,512]{1,0:T(8,128)(2,1)S(1)} %convolution_convert_fusion.3), channel_id=2, replica_groups=mesh['kv'=8,'tp'=4] {'tp'}, dimensions={0}, use_global_device_ids=true | all-gather | bytes 163840 | tf_op jit(solution)/shard_map/all_gather | solution.py:12
  136.3 1.6 convolution_convert_fusion
  138.0 1.6 convolution_convert_fusion.1
  139.6 20.6 %psum.22 = bf16[32]{0:T(256)(128)(2,1)S(1)} all-reduce(bf16[32]{0:T(256)(128)(2,1)S(1)} %get-tuple-element.11), channel_id=1, replica_groups=mesh['kv'=8,'tp'=4] {'kv'}, use_global_device_ids=true, to_apply=%region_14.15 | all-reduce | flops 32 | bytes 128 | tf_op jit(solution)/shard_map/psum | solution.py:159
  160.2 51.3 %all-reduce.13.cloned.1.call-done = (bf16[32,2752]{1,0:T(8,128)(2,1)}, bf16[32,2752]{1,0:T(8,128)(2,1)}) async-done(((bf16[32,2752]{1,0:T(8,128)(2,1)}, bf16[32,2752]{1,0:T(8,128)(2,1)}), (bf16[32,2752]{1,0:T(8,128)(2,1)}, bf16[32,2752]{1,0:T(8,128)(2,1)})) %all-reduce.13.cloned.1.call-update) | async-done | bytes 352272 | tf_op jit(solution)/shard_map/psum | solution.py:158
  211.6 2.6 %convolution_convert_fusion.2 = bf16[32,512]{1,0:T(8,128)(2,1)S(1)} fusion(bf16[2752,512]{1,0:T(8,128)(2,1)} %param.39, bf16[32,2752]{1,0:T(8,128)(2,1)} %get-tuple-element.9, bf16[32,2752]{1,0:T(8,128)(2,1)} %get-tuple-element.10, f32[32]{0:T(128)S(1)} %add_rsqrt_fusion.1), kind=kOutput, calls=%fused_computation.2 | convolution fusion | flops 91074560 | bytes 3203200 | tf_op jit(solution)/shard_map/dot_general | solution.py:162
  214.2 5.4 %all-gather.1 = bf16[128,512]{1,0:T(8,128)(2,1)S(1)} all-gather(bf16[32,512]{1,0:T(8,128)(2,1)S(1)} %convolution_convert_fusion.2), channel_id=3, replica_groups=mesh['kv'=8,'tp'=4] {'tp'}, dimensions={0}, use_global_device_ids=true | all-gather | bytes 163840 | tf_op jit(solution)/shard_map/all_gather | solution.py:12
  (44 shorter events, 3.0 us)
Async XLA Ops:
  7.2 129.1 %copy-start = (bf16[512,2752]{0,1:T(8,128)(2,1)S(1)}, bf16[512,2752]{0,1:T(8,128)(2,1)}, u32[]{:S(2)}) copy-start(bf16[512,2752]{0,1:T(8,128)(2,1)} %param.38) | copy-start | bytes 8454148
  7.2 15.7 %copy-start.2 = (f32[4,64,2,128]{3,2,1,0:T(2,128)S(1)}, f32[4,64,2,128]{3,2,1,0:T(2,128)}, u32[]{:S(2)}) copy-start(f32[4,64,2,128]{3,2,1,0:T(2,128)} %param.32) | copy-start | bytes 786436
  7.2 85.3 %copy-start.9 = (f32[256]{0:T(256)S(1)}, f32[256]{0:T(256)}, u32[]{:S(2)}) copy-start(f32[256]{0:T(256)} %param.28) | copy-start | bytes 3076
  7.2 85.3 %copy-start.8 = (bf16[16,256]{1,0:T(8,128)(2,1)S(1)}, bf16[16,256]{1,0:T(8,128)(2,1)}, u32[]{:S(2)}) copy-start(bf16[16,256]{1,0:T(8,128)(2,1)} %param.27) | copy-start | bytes 24580
  7.2 91.5 %copy-start.7 = (f32[256]{0:T(256)S(1)}, f32[256]{0:T(256)}, u32[]{:S(2)}) copy-start(f32[256]{0:T(256)} %param.29) | copy-start | bytes 3076
  7.2 84.6 %all-reduce.11.cloned.1.call-start = ((), (), s32[]{:S(2)}) async-start(), calls=%async_computation | async-start | bytes 214016
  12.0 124.1 %copy-start.3 = (bf16[32,512]{1,0:T(8,128)(2,1)S(1)}, bf16[32,512]{1,0:T(8,128)(2,1)}, u32[]{:S(2)}) copy-start(bf16[32,512]{1,0:T(8,128)(2,1)} %param.20) | copy-start | bytes 98308
  13.8 122.5 %copy-start.6 = (f32[512]{0:T(512)S(1)}, f32[512]{0:T(512)}, u32[]{:S(2)}) copy-start(f32[512]{0:T(512)} %param.36) | copy-start | bytes 6148
  17.6 194.0 %all-reduce.13.cloned.1.call-start = ((), (), s32[]{:S(2)}) async-start(), calls=%async_computation.1 | async-start | bytes 720896 | tf_op jit(solution)/shard_map/psum | solution.py:158
  94.2 43.7 %copy-start.5 = (bf16[4,2,128]{2,1,0:T(2,128)(2,1)}, bf16[4,2,128]{2,1,0:T(2,128)(2,1)S(1)}, u32[]{:S(2)}) copy-start(bf16[4,2,128]{2,1,0:T(2,128)(2,1)S(1)} %reshape.74) | copy-start | bytes 6148
  95.0 42.9 %copy-start.4 = (bf16[4,2,256]{2,1,0:T(2,128)(2,1)}, bf16[4,2,256]{2,1,0:T(2,128)(2,1)S(1)}, u32[]{:S(2)}) copy-start(bf16[4,2,256]{2,1,0:T(2,128)(2,1)S(1)} %reshape.75) | copy-start | bytes 12292
  136.2 1.8 copy-start.1
Sparse Core Ops, SparseCore 0:
  17.7 74.0 all-reduce.10
  139.7 71.7 all-reduce.12
